TPU v7x, 32 devices: a whole 2x2x4 slice. The times are simulated.
32 devices in a mesh: fs: 4 (over y, x), tp: 8 (over z, core).
Axes of the slice: x: 2, y: 2, z: 4, core: 2. Of those that a mesh axis runs over, the one named last changes fastest.
Arguments:
- tokens: bfloat16 [512, 4096], P('fs', 'tp'), may hold values from -6 to 6
- expert_ids: int32 [512, 8], P('fs'), may hold values from 0 to 63, all different within a row; in each aligned block of 128 rows (0 to 127, 128 to 255, ...) at most 32 rows name the same one
- affinity: float32 [512, 8], P('fs'), may hold values from 0.05 to 1
- norm_gain: float32 [4096], P('fs'), may hold values from 0.1 to 1.9
- gate_train: float32 [64, 512, 4096], P(None, 'tp', 'fs'), may hold values from -0.09375 to 0.09375
- up_train: float32 [64, 512, 4096], P(None, 'tp', 'fs'), may hold values from -0.09375 to 0.09375
- down_train: float32 [64, 512, 4096], P(None, 'fs', 'tp'), may hold values from -0.25 to 0.25
- shared_gate_train: float32 [512, 4096], P('tp', 'fs'), may hold values from -0.09375 to 0.09375
- shared_up_train: float32 [512, 4096], P('tp', 'fs'), may hold values from -0.09375 to 0.09375
- shared_down_train: float32 [512, 4096], P('fs', 'tp'), may hold values from -0.25 to 0.25
Outputs:
- mixed: bfloat16 [512, 4096], P('fs', 'tp')
- gate_serve: bfloat16 [64, 512, 4096], P('fs', 'tp')
- up_serve: bfloat16 [64, 512, 4096], P('fs', 'tp')
- down_serve: bfloat16 [64, 512, 4096], P('fs', None, 'tp')
- shared_gate_serve: bfloat16 [512, 4096], P('tp')
- shared_up_serve: bfloat16 [512, 4096], P('tp')
- shared_down_serve: bfloat16 [512, 4096], P(None, 'tp')
Inputs may be any that keep to these rules, and one draw needn't show every extreme that they name: `expert_ids`: each row names 8 different experts. In each aligned block of 128 rows (the tokens of one index of fs) no expert is named by more than 32 rows, a bound that some block reaches.
All inputs are finite; a program needn't handle non-finite values.
Results may differ from a plain program's by a relative error of at most 0.019.
Values may be sent and summed in bfloat16 or wider, within the bound.
A program may use at most 192 MiB of HBM per device.

v0:
```python
import jax
import jax.numpy as jnp
from jax import lax
from jax.sharding import PartitionSpec as P

EXPERTS = 64
K = 8
CAP = 32


norm_eps = 1e-06
routed_scale = 2.5


def body(
    tokens,
    expert_ids,
    affinity,
    norm_gain,
    gate_train,
    up_train,
    down_train,
    shared_gate_train,
    shared_up_train,
    shared_down_train,
):
    gain_cols = norm_gain[None, None, :]
    gate_send = (gate_train * gain_cols).astype(jnp.bfloat16)
    up_send = (up_train * gain_cols).astype(jnp.bfloat16)
    down_send = down_train.astype(jnp.bfloat16)
    shared_gate_serve, shared_up_serve, shared_down_serve = (
        lax.all_gather(
            (shared_gate_train * norm_gain[None, :]).astype(jnp.bfloat16), "fs", axis=1, tiled=True
        ),
        lax.all_gather(
            (shared_up_train * norm_gain[None, :]).astype(jnp.bfloat16), "fs", axis=1, tiled=True
        ),
        lax.all_gather(shared_down_train.astype(jnp.bfloat16), "fs", axis=0, tiled=True),
    )
    gate_serve, up_serve = (
        lax.all_to_all(gate_send, "fs", split_axis=0, concat_axis=2, tiled=True),
        lax.all_to_all(up_send, "fs", split_axis=0, concat_axis=2, tiled=True),
    )
    full_rows = lax.all_gather(tokens, "tp", axis=1, tiled=True)
    widened = full_rows.astype(jnp.float32)
    inverse_rms = lax.rsqrt(jnp.mean(widened * widened, axis=1) + norm_eps)
    shared_gate = (
        jnp.einsum("td,hd->th", full_rows, shared_gate_serve, preferred_element_type=jnp.float32)
        * inverse_rms[:, None]
    )
    shared_up = (
        jnp.einsum("td,hd->th", full_rows, shared_up_serve, preferred_element_type=jnp.float32)
        * inverse_rms[:, None]
    )
    shared_hidden = (jax.nn.silu(shared_gate) * shared_up).astype(jnp.bfloat16)
    token_count = tokens.shape[0]
    flat_ids = expert_ids.reshape(-1)
    onehot = (flat_ids[:, None] == jnp.arange(EXPERTS, dtype=jnp.int32)[None, :]).astype(jnp.int32)
    slot_index = jnp.sum((jnp.cumsum(onehot, axis=0) - onehot) * onehot, axis=1)
    position = flat_ids * CAP + slot_index
    token_of = jnp.repeat(jnp.arange(token_count, dtype=jnp.int32), K)
    row_scale = (
        jnp.zeros((EXPERTS * CAP,), jnp.float32)
        .at[position]
        .set(inverse_rms[token_of])
        .reshape(EXPERTS, CAP)
    )
    outgoing = (
        jnp.zeros((EXPERTS * CAP, tokens.shape[1]), jnp.bfloat16).at[position].set(tokens[token_of])
    )
    strips, arrived_scale = (
        lax.all_to_all(
            outgoing.reshape(EXPERTS, CAP, -1), "fs", split_axis=0, concat_axis=1, tiled=True
        ),
        lax.all_to_all(
            row_scale.astype(jnp.bfloat16), "fs", split_axis=0, concat_axis=1, tiled=True
        ).astype(row_scale.dtype),
    )
    piece = lax.all_gather(strips, "tp", axis=2, tiled=True)
    gate_pre = jnp.einsum("erd,ehd->erh", piece, gate_serve, preferred_element_type=jnp.float32)
    up_pre = jnp.einsum("erd,ehd->erh", piece, up_serve, preferred_element_type=jnp.float32)
    routed_hidden = (
        jax.nn.silu(gate_pre * arrived_scale[:, :, None]) * (up_pre * arrived_scale[:, :, None])
    ).astype(jnp.bfloat16)
    down_serve = lax.all_to_all(down_send, "fs", split_axis=0, concat_axis=1, tiled=True)
    shared_out = jnp.einsum(
        "brh,hd->brd",
        lax.all_gather(shared_hidden[None], "tp", axis=2, tiled=True),
        shared_down_serve,
        preferred_element_type=jnp.float32,
    )
    routed_out = jnp.einsum(
        "erh,ehd->erd",
        lax.all_gather(routed_hidden, "tp", axis=2, tiled=True),
        down_serve,
        preferred_element_type=jnp.float32,
    )
    returned = lax.all_to_all(
        routed_out.astype(jnp.bfloat16), "fs", split_axis=1, concat_axis=0, tiled=True
    )
    picked = (
        returned.reshape(EXPERTS * CAP, -1)[position]
        .reshape(token_count, K, -1)
        .astype(jnp.float32)
    )
    route_weight = routed_scale * affinity / jnp.sum(affinity, axis=1, keepdims=True)
    routed = jnp.sum(picked * route_weight[:, :, None], axis=1)
    mixed_out = (shared_out[0] + routed).astype(jnp.bfloat16)
    return (
        mixed_out,
        gate_serve,
        up_serve,
        down_serve,
        shared_gate_serve,
        shared_up_serve,
        shared_down_serve,
    )


def solution(mesh):
    return jax.shard_map(
        body,
        mesh=mesh,
        in_specs=(
            P("fs", "tp"),
            P("fs", None),
            P("fs", None),
            P("fs"),
            P(None, "tp", "fs"),
            P(None, "tp", "fs"),
            P(None, "fs", "tp"),
            P("tp", "fs"),
            P("tp", "fs"),
            P("fs", "tp"),
        ),
        out_specs=(
            P("fs", "tp"),
            P("fs", "tp", None),
            P("fs", "tp", None),
            P("fs", None, "tp"),
            P("tp", None),
            P("tp", None),
            P(None, "tp"),
        ),
        check_vma=False,
    )
```

profile of v0, /device:TPU:0, one launch (start us, length us, event | category | flops | bytes accessed | tf_op | source)
XLA Modules:
  0.0 509.5 jit_solution(12004275451097814454)
XLA Ops:
  7.2 0.7 all-gather.5.cloned.1.call-update
  7.9 0.7 broadcast_multiply_fusion
  8.6 0.8 copy.46
  9.6 18.0 %reduce-window.6 = s32[64,8,128]{2,1,0:T(8,128)S(1)} reduce-window(s32[64,8,128]{2,1,0:T(8,128)S(1)} %fusion.14, s32[]{:T(128)} %constant.8.clone.1), window={size=1x1x128 pad=0_0x0_0x127_0}, to_apply=%region_1.2 | reduce-window | flops 8323072 | bytes 524292 | tf_op jit(solution)/shard_map/reduce-window
  27.6 0.1 slice.14
  27.8 0.1 copy.48
  28.1 0.1 broadcast_add_fusion
  28.6 13.4 %scatter_custom_fusion = bf16[2048,512]{1,0:T(8,128)(2,1)S(1)} fusion(s32[1024]{0:T(1024)S(1)} %bitcast.80, bf16[128,512]{1,0:T(8,128)(2,1)} %param.10, s32[1024]{0:T(1024)S(1)} %broadcast_clamp_fusion.1, bf16[]{:T(256)} %constant.7.clone.1), kind=kCustom, calls=%fused_computation.25 | custom fusion | bytes 2097664 | tf_op jit(solution)/shard_map/scatter | solution.py:69
  42.0 30.4 %all_to_all.97 = bf16[64,32,512]{2,1,0:T(8,128)(2,1)S(1)} all-to-all(bf16[64,32,512]{2,1,0:T(8,128)(2,1)S(1)} %bitcast.75), channel_id=1, replica_groups=mesh['fs'=4,'tp'=8] {'fs'}, dimensions={0} | all-to-all | bytes 4194304 | tf_op jit(solution)/shard_map/all_to_all | solution.py:72
  72.4 1.6 copy.50
  74.0 1.5 multiply_reduce_fusion
  75.6 6.6 %gather_fusion = f32[1024]{0:T(1024)S(1)} fusion(f32[128]{0:T(128)S(1)} %add_rsqrt_fusion, s32[1024]{0:T(1024)S(1)} %broadcast_clamp_fusion.1), kind=kCustom, calls=%fused_computation.1 | custom fusion | bytes 12288 | tf_op jit(solution)/shard_map/gather | solution.py:65
  82.1 4.3 scatter_custom_fusion.1
  86.5 0.7 reshape.187
  87.2 3.2 all-to-all-start.2
  90.5 17.9 %multiply_convert_fusion.1 = (bf16[64,64,1024]{2,1,0:T(8,128)(2,1)}, bf16[64,64,1024]{2,1,0:T(8,128)(2,1)}) fusion(f32[64,64,1024]{2,1,0:T(8,128)} %param.14, f32[1024]{0:T(1024)S(1)} %copy-done.7, f32[64,64,1024]{2,1,0:T(8,128)} %param.15), kind=kLoop, calls=%fused_computation.6 | loop fusion | flops 16777216 | bytes 50335744 | tf_op jit(solution)/shard_map/convert_element_type | solution.py:28
  108.4 99.5 %all_to_all.98 = bf16[64,64,1024]{2,1,0:T(8,128)(2,1)} all-to-all(bf16[64,64,1024]{2,1,0:T(8,128)(2,1)} %get-tuple-element.10), channel_id=1, replica_groups=mesh['fs'=4,'tp'=8] {'fs'}, dimensions={0} | all-to-all | bytes 16777216 | tf_op jit(solution)/shard_map/all_to_all | solution.py:42
  207.9 5.8 %all-to-all-start.1 = ((bf16[64,64,1024]{2,1,0:T(8,128)(2,1)}), bf16[64,64,1024]{2,1,0:T(8,128)(2,1)}, u32[]{:S(2)}, u32[]{:S(2)}) async-start(bf16[64,64,1024]{2,1,0:T(8,128)(2,1)} %get-tuple-element.9), calls=%async_computation.1 | async-start | bytes 16777216 | tf_op jit(solution)/shard_map/all_to_all | solution.py:41
  213.7 9.1 %convert_element_type.81 = bf16[64,128,512]{2,1,0:T(8,128)(2,1)} convert(f32[64,128,512]{2,1,0:T(8,128)} %param.16) | non-fusion elementwise | flops 4194304 | bytes 25165824 | tf_op jit(solution)/shard_map/convert_element_type | solution.py:30
  223.0 11.1 %copy.62 = bf16[4,16,64,1024]{3,0,2,1:T(4,128)(2,1)} copy(bf16[4,16,64,1024]{3,2,1,0:T(8,128)(2,1)} %bitcast.70) | data formatting | bytes 16777216 | tf_op jit(solution)/shard_map/all_to_all | solution.py:42
  234.0 14.3 %all_to_all.83 = bf16[16,64,4096]{2,1,0:T(8,128)(2,1)} reshape(bf16[16,64,4,1024]{3,2,1,0:T(4,128)(2,1)} %bitcast.71) | data formatting | bytes 16777216 | tf_op jit(solution)/shard_map/all_to_all | solution.py:42
  248.4 55.3 %all-to-all-done.1 = bf16[64,64,1024]{2,1,0:T(8,128)(2,1)} async-done(((bf16[64,64,1024]{2,1,0:T(8,128)(2,1)}), bf16[64,64,1024]{2,1,0:T(8,128)(2,1)}, u32[]{:S(2)}, u32[]{:S(2)}) %all-to-all-start.1) | async-done | bytes 8388640 | tf_op jit(solution)/shard_map/all_to_all | solution.py:41
  303.7 5.7 %all-to-all-start.4 = ((bf16[64,128,512]{2,1,0:T(8,128)(2,1)}), bf16[64,128,512]{2,1,0:T(8,128)(2,1)}, u32[]{:S(2)}, u32[]{:S(2)}) async-start(bf16[64,128,512]{2,1,0:T(8,128)(2,1)} %convert_element_type.81), calls=%async_computation.4 | async-start | bytes 16777216 | tf_op jit(solution)/shard_map/all_to_all | solution.py:85
  309.4 11.1 %copy.63 = bf16[4,16,64,1024]{3,0,2,1:T(4,128)(2,1)} copy(bf16[4,16,64,1024]{3,2,1,0:T(8,128)(2,1)} %bitcast.11) | data formatting | bytes 16777216 | tf_op jit(solution)/shard_map/all_to_all | solution.py:41
  320.5 14.3 %all_to_all.78 = bf16[16,64,4096]{2,1,0:T(8,128)(2,1)} reshape(bf16[16,64,4,1024]{3,2,1,0:T(4,128)(2,1)} %bitcast.72) | data formatting | bytes 16777216 | tf_op jit(solution)/shard_map/all_to_all | solution.py:41
  334.9 11.2 %convolution_multiply_fusion.1 = f32[16,128,64]{1,2,0:T(8,128)S(1)} fusion(bf16[16,128,4096]{2,1,0:T(8,128)(2,1)} %all-gather.7.cloned.1.call-done, bf16[16,64,4096]{2,1,0:T(8,128)(2,1)} %all_to_all.78, f32[16,128]{1,0:T(8,128)S(1)} %reshape.135), kind=kOutput, calls=%fused_computation.14 | convolution fusion | flops 1073872896 | bytes 25698304 | tf_op jit(solution)/shard_map/erd,ehd->erh/dot_general | solution.py:80
  346.1 12.0 %fusion.2 = bf16[16,128,64]{1,2,0:T(8,128)(2,1)} fusion(bf16[16,128,4096]{2,1,0:T(8,128)(2,1)} %all-gather.7.cloned.1.call-done, bf16[16,64,4096]{2,1,0:T(8,128)(2,1)} %all_to_all.83, f32[16,128,64]{1,2,0:T(8,128)S(1)} %convolution_multiply_fusion.1, f32[16,128]{1,0:T(8,128)S(1)} %reshape.135), kind=kOutput, calls=%fused_computation.16 | convolution fusion | flops 1074659328 | bytes 25960448 | tf_op jit(solution)/shard_map/erd,ehd->erh/dot_general | solution.py:81
  358.2 43.1 %all-to-all-done.4 = bf16[64,128,512]{2,1,0:T(8,128)(2,1)} async-done(((bf16[64,128,512]{2,1,0:T(8,128)(2,1)}), bf16[64,128,512]{2,1,0:T(8,128)(2,1)}, u32[]{:S(2)}, u32[]{:S(2)}) %all-to-all-start.4) | async-done | bytes 8388640 | tf_op jit(solution)/shard_map/all_to_all | solution.py:85
  401.3 7.8 %copy.54 = bf16[4,16,128,512]{3,2,0,1:T(8,128)(2,1)} copy(bf16[4,16,128,512]{3,2,1,0:T(8,128)(2,1)} %bitcast.16) | data formatting | bytes 16777216 | tf_op jit(solution)/shard_map/all_to_all | solution.py:85
  409.0 5.4 %convolution_convert_fusion = bf16[16,128,512]{2,1,0:T(8,128)(2,1)S(1)} fusion(bf16[16,128,512]{1,2,0:T(8,128)(2,1)} %all-gather.9.cloned.1.call-done, bf16[16,512,512]{2,1,0:T(8,128)(2,1)} %bitcast.67), kind=kOutput, calls=%fused_computation.12 | convolution fusion | flops 1074790400 | bytes 12582912 | tf_op jit(solution)/shard_map/erh,ehd->erd/dot_general | solution.py:92
  414.5 2.5 copy.55
  417.0 3.6 all-to-all-start.5
  420.7 1.0 convert_element_type.70
  421.7 1.0 multiply_convert_fusion.3
  422.7 28.5 %all_gather.21 = bf16[64,4096]{1,0:T(8,128)(2,1)S(1)} all-gather(bf16[64,1024]{1,0:T(8,128)(2,1)S(1)} %get-tuple-element.7), channel_id=1, replica_groups=mesh['fs'=4,'tp'=8] {'fs'}, dimensions={1}, use_global_device_ids=true | all-gather | bytes 655360 | tf_op jit(solution)/shard_map/all_gather | solution.py:32
  451.2 9.4 %all_gather.23 = bf16[64,4096]{1,0:T(8,128)(2,1)S(1)} all-gather(bf16[64,1024]{1,0:T(8,128)(2,1)S(1)} %get-tuple-element.8), channel_id=1, replica_groups=mesh['fs'=4,'tp'=8] {'fs'}, dimensions={1}, use_global_device_ids=true | all-gather | bytes 655360 | tf_op jit(solution)/shard_map/all_gather | solution.py:35
  460.5 10.9 %all_gather.25 = bf16[512,512]{1,0:T(8,128)(2,1)} all-gather(bf16[128,512]{1,0:T(8,128)(2,1)S(1)} %convert_element_type.70), channel_id=1, replica_groups=mesh['fs'=4,'tp'=8] {'fs'}, dimensions={0}, use_global_device_ids=true | all-gather | bytes 655360 | tf_op jit(solution)/shard_map/all_gather | solution.py:38
  471.4 0.5 fusion.6
  471.9 0.5 fusion.7
  472.4 14.0 %all-gather = bf16[128,512]{0,1:T(8,128)(2,1)S(1)} all-gather(bf16[128,64]{0,1:T(8,128)(2,1)S(1)} %fusion.7), channel_id=2, replica_groups=mesh['fs'=4,'tp'=8] {'tp'}, dimensions={1}, use_global_device_ids=true | all-gather | bytes 147456 | tf_op jit(solution)/shard_map/all_gather | solution.py:88
  486.4 1.4 copy-done.1
  487.7 2.8 copy.56
  490.6 5.1 gather_fusion.1
  495.7 1.9 fusion
  497.6 2.0 fusion.3
  499.6 0.8 copy.67
  500.3 0.8 copy.68
  501.1 1.9 copy.69
  (52 shorter events, 1.4 us)
Async XLA Ops:
  7.2 66.9 %all-gather.5.cloned.1.call-start = ((), (), s32[]{:S(2)}) async-start(), calls=%async_computation.6 | async-start | bytes 1179648 | tf_op jit(solution)/shard_map/all_gather | solution.py:44
  7.9 327.0 %all-gather.7.cloned.1.call-start = ((), (), s32[]{:S(2)}) async-start(), calls=%async_computation.7 | async-start | bytes 18874368 | tf_op jit(solution)/shard_map/all_gather | solution.py:79
  42.0 48.5 %copy-start.7 = (f32[1024]{0:T(1024)S(1)}, f32[1024]{0:T(1024)}, u32[]{:S(2)}) copy-start(f32[1024]{0:T(1024)} %param.13) | copy-start | bytes 12292
  87.2 21.2 %all-to-all-start.2 = ((bf16[4,2,256]{2,1,0:T(2,128)(2,1)}), bf16[4,2,256]{2,1,0:T(2,128)(2,1)S(1)}, u32[]{:S(2)}, u32[]{:S(2)}) async-start(bf16[4,2,256]{2,1,0:T(2,128)(2,1)} %reshape.187), calls=%async_computation.2 | async-start | bytes 8192 | tf_op jit(solution)/shard_map/all_to_all | solution.py:75
  207.9 95.9 %all-to-all-start.1 = ((bf16[64,64,1024]{2,1,0:T(8,128)(2,1)}), bf16[64,64,1024]{2,1,0:T(8,128)(2,1)}, u32[]{:S(2)}, u32[]{:S(2)}) async-start(bf16[64,64,1024]{2,1,0:T(8,128)(2,1)} %get-tuple-element.9), calls=%async_computation.1 | async-start | bytes 16777216 | tf_op jit(solution)/shard_map/all_to_all | solution.py:41
  303.7 97.5 %all-to-all-start.4 = ((bf16[64,128,512]{2,1,0:T(8,128)(2,1)}), bf16[64,128,512]{2,1,0:T(8,128)(2,1)}, u32[]{:S(2)}, u32[]{:S(2)}) async-start(bf16[64,128,512]{2,1,0:T(8,128)(2,1)} %convert_element_type.81), calls=%async_computation.4 | async-start | bytes 16777216 | tf_op jit(solution)/shard_map/all_to_all | solution.py:85
  309.4 99.6 %all-gather.9.cloned.1.call-start = ((), (), s32[]{:S(2)}) async-start(), calls=%async_computation.8 | async-start | bytes 2359296 | tf_op jit(solution)/shard_map/all_gather | solution.py:94
  346.1 12.1 %copy-start.8 = (f32[128,8]{0,1:T(8,128)S(1)}, f32[128,8]{0,1:T(8,128)}, u32[]{:S(2)}) copy-start(f32[128,8]{0,1:T(8,128)} %param.12) | copy-start | bytes 12292
  414.5 7.2 %copy-start.6 = (f32[64,1024]{1,0:T(8,128)S(1)}, f32[64,1024]{1,0:T(8,128)}, u32[]{:S(2)}) copy-start(f32[64,1024]{1,0:T(8,128)} %param.17) | copy-start | bytes 786436
  414.5 56.9 %copy-start = (bf16[128,4096]{1,0:T(8,128)(2,1)S(1)}, bf16[128,4096]{1,0:T(8,128)(2,1)}, u32[]{:S(2)}) copy-start(bf16[128,4096]{1,0:T(8,128)(2,1)} %all-gather.5.cloned.1.call-done) | copy-start | bytes 3145732
  417.0 69.4 %all-to-all-start.5 = ((bf16[16,128,512]{2,0,1:T(8,128)(2,1)}), bf16[16,128,512]{2,0,1:T(8,128)(2,1)S(1)}, u32[]{:S(2)}, u32[]{:S(2)}) async-start(bf16[16,128,512]{2,0,1:T(8,128)(2,1)} %copy.55), calls=%async_computation.5 | async-start | bytes 4194304 | tf_op jit(solution)/shard_map/all_to_all | solution.py:98
  451.2 21.2 %copy-start.2 = (bf16[64,4096]{1,0:T(8,128)(2,1)}, bf16[64,4096]{1,0:T(8,128)(2,1)S(1)}, u32[]{:S(2)}) copy-start(bf16[64,4096]{1,0:T(8,128)(2,1)S(1)} %all_gather.21) | copy-start | bytes 1572868
  460.5 11.9 %copy-start.4 = (bf16[64,4096]{1,0:T(8,128)(2,1)}, bf16[64,4096]{1,0:T(8,128)(2,1)S(1)}, u32[]{:S(2)}) copy-start(bf16[64,4096]{1,0:T(8,128)(2,1)S(1)} %all_gather.23) | copy-start | bytes 1572868
  486.4 1.4 copy-start.1
  487.7 11.8 %copy-start.3 = (bf16[64,4096]{1,0:T(8,128)(2,1)S(1)}, bf16[64,4096]{1,0:T(8,128)(2,1)}, u32[]{:S(2)}) copy-start(bf16[64,4096]{1,0:T(8,128)(2,1)} %copy-done.2) | copy-start | bytes 1572868
  487.7 12.6 %copy-start.5 = (bf16[64,4096]{1,0:T(8,128)(2,1)S(1)}, bf16[64,4096]{1,0:T(8,128)(2,1)}, u32[]{:S(2)}) copy-start(bf16[64,4096]{1,0:T(8,128)(2,1)} %copy-done.4) | copy-start | bytes 1572868
Sparse Core Ops, SparseCore 0:
  9.6 24.8 all-gather.4
  74.1 150.7 all-gather.6
  358.2 30.6 all-gather.8
where the time goes:
time: 511 us; the launch traced here: 510 us
  blocking collectives  192 us (38%)
  local copies, waits for them, and re-layouts  102 us (20%)
  waiting for transfers between devices  99.2 us (19%)
  other arithmetic  51.4 us (10%)
  matrix products  31.6 us (6%)
  starting transfers between devices  18.5 us (4%)
  between operations  14 us (3%)
    all_to_all x1, blocking collectives, body(): lax.all_to_all(up_send, 'fs', split_axis=0, concat_axis=2, tiled=True)  99.5 us
    all_to_all x1, waiting for transfers between devices, body(): lax.all_to_all(gate_send, 'fs', split_axis=0, concat_axis=2, tiled=True)  55.3 us
    all_to_all x1, waiting for transfers between devices, body(): lax.all_to_all(down_send, 'fs', split_axis=0, concat_axis=1, tiled=True)  43.1 us
    all_to_all x1, blocking collectives, body(): lax.all_to_all(outgoing.reshape(EXPERTS, CAP, -1), 'fs', split_axis=0, co...  30.4 us
    all_gather x1, blocking collectives, body(): lax.all_gather((shared_gate_train * norm_gain[None, :]).astype(jnp.bfloat...  28.5 us
    all_to_all x2, local copies, waits for them, and re-layouts, body(): lax.all_to_all(gate_send, 'fs', split_axis=0, concat_axis=2, tiled=True)  25.4 us
    all_to_all x2, local copies, waits for them, and re-layouts, body(): lax.all_to_all(up_send, 'fs', split_axis=0, concat_axis=2, tiled=True)  25.4 us
    another operation x3, other arithmetic  18.2 us
  transfers between devices with their start and end apart: 7, of which 2 were waited for; matrix products, arithmetic and copies ran while one was open for 26% of the time, Pallas kernels for 0%

commit v1 on v0

v1 whole, which is shorter than its diff:
```python
import functools

import jax
import jax.numpy as jnp
from jax import lax
from jax.experimental import pallas as pl
from jax.experimental.pallas import tpu as pltpu
from jax.sharding import PartitionSpec as P

MESH = pl.DeviceIdType.MESH

norm_eps = 1e-06
routed_scale = 2.5


def exchange_kernel(n, specs, nsmall, *refs):
    nw = len(specs)
    nbig = nw - nsmall
    ins = refs[:nw]
    gain_ref = refs[nw]
    outs = refs[nw + 1 : 2 * nw + 1]
    scr = list(refs[2 * nw + 1 :])
    fbuf, lsem, ssem, rsem, osem = scr[:5]
    bufs = scr[5:]
    me = lax.axis_index("fs")
    dest = [lax.rem(me + k, n) for k in range(n)]

    barrier = pltpu.get_barrier_semaphore()
    for k in range(1, n):
        pl.semaphore_signal(barrier, inc=1, device_id={"fs": dest[k]}, device_id_type=MESH)
    pl.semaphore_wait(barrier, n - 1)

    def place(w, who, first, count):
        cut, _ = specs[w]
        width = ins[w].shape[cut]
        part = pl.ds(pl.multiple_of(who * width, width), width)
        if w >= nbig:
            return outs[w].at[part, :] if cut == 0 else outs[w].at[:, part]
        if cut == 1:
            return outs[w].at[pl.ds(first, count), part, :]
        return outs[w].at[pl.ds(first, count), :, part]

    def remote(w, k, src, first, count):
        return pltpu.make_async_remote_copy(
            src_ref=src,
            dst_ref=place(w, me, first, count),
            send_sem=ssem.at[w, k],
            recv_sem=rsem.at[w, k],
            device_id={"fs": dest[k]},
            device_id_type=MESH,
        )

    small = range(nbig, nw)
    for w in small:
        pltpu.make_async_copy(ins[w], bufs[nw + w - nbig], osem.at[w]).start()
    order = list(range(1, n)) + [0]
    for w in range(nbig):
        cut, scaled = specs[w]
        local = outs[w].shape[0]
        chunk = fbuf.shape[1]
        shape = ins[w].shape[1:]
        steps = local // chunk
        view = fbuf if fbuf.shape[2:] == shape else None
        assert view is not None

        def load(j, k, w=w, local=local, chunk=chunk):
            return pltpu.make_async_copy(
                ins[w].at[pl.ds(dest[k] * local + j * chunk, chunk)], fbuf.at[k], lsem.at[k]
            )

        for k in order:
            load(0, k).start()
        if w == 0:
            for s in small:
                pltpu.make_async_copy(ins[s], bufs[nw + s - nbig], osem.at[s]).wait()
                value = bufs[nw + s - nbig][...]
                if specs[s][1]:
                    value = value * gain_ref[...]
                bufs[s][...] = value.astype(jnp.bfloat16)

        def step(j, carry, w=w, chunk=chunk, steps=steps, scaled=scaled, load=load):
            first = j * chunk
            pending = None
            for k in order:
                load(j, k).wait()
                for c in range(chunk):
                    value = fbuf[k, c]
                    if scaled:
                        value = value * gain_ref[...]
                    bufs[w][k, first + c] = value.astype(jnp.bfloat16)

                @pl.when(j + 1 < steps)
                def _():
                    load(j + 1, k).start()

                if pending is not None:
                    remote(w, pending, bufs[w].at[pending, pl.ds(first, chunk)], first, chunk).start()
                pending = k
            pltpu.make_async_copy(
                bufs[w].at[0, pl.ds(first, chunk)], place(w, me, first, chunk), osem.at[w]
            ).start()
            return carry

        lax.fori_loop(0, steps, step, 0)
    for s in small:
        for k in order[:-1]:
            remote(s, k, bufs[s], 0, 0).start()
        pltpu.make_async_copy(bufs[s], place(s, me, 0, 0), osem.at[s]).start()

    for w in range(nw):
        big = w < nbig
        local = outs[w].shape[0] if big else 0
        for k in range(1, n):
            src = bufs[w].at[k] if big else bufs[w]
            source = lax.rem(me + n - k, n)
            pltpu.make_async_remote_copy(
                src_ref=src,
                dst_ref=place(w, source, 0, local),
                send_sem=ssem.at[w, k],
                recv_sem=rsem.at[w, k],
                device_id={"fs": dest[k]},
                device_id_type=MESH,
            ).wait()
        own = bufs[w].at[0] if big else bufs[w]
        pltpu.make_async_copy(own, place(w, me, 0, local), osem.at[w]).wait()


def exchange(n, weights, smalls, gain, collective_id):
    both = weights + smalls
    outs, bufs = [], []
    for a, cut, _ in weights:
        dims = list(a.shape)
        dims[0] //= n
        bufs.append(pltpu.VMEM((n, *dims), jnp.bfloat16))
        dims[cut] *= n
        outs.append(jax.ShapeDtypeStruct(tuple(dims), jnp.bfloat16))
    for a, cut, _ in smalls:
        dims = list(a.shape)
        bufs.append(pltpu.VMEM(tuple(dims), jnp.bfloat16))
        dims[cut] *= n
        outs.append(jax.ShapeDtypeStruct(tuple(dims), jnp.bfloat16))
    for a, _, _ in smalls:
        bufs.append(pltpu.VMEM(a.shape, jnp.float32))
    local = weights[0][0].shape[0] // n
    chunk = 2 if local % 2 == 0 else 1
    sent = sum(2 * a.size * (n - 1) // n for a, _, _ in weights)
    nw = len(both)
    any_spec = pl.BlockSpec(memory_space=pl.ANY)
    return pl.pallas_call(
        functools.partial(exchange_kernel, n, [(c, g) for _, c, g in both], len(smalls)),
        out_shape=tuple(outs),
        in_specs=[any_spec] * nw + [pl.BlockSpec(memory_space=pltpu.VMEM)],
        out_specs=(any_spec,) * nw,
        scratch_shapes=[
            pltpu.VMEM((n, chunk, *weights[0][0].shape[1:]), jnp.float32),
            pltpu.SemaphoreType.DMA((n,)),
            pltpu.SemaphoreType.DMA((nw, n)),
            pltpu.SemaphoreType.DMA((nw, n)),
            pltpu.SemaphoreType.DMA((nw,)),
            *bufs,
        ],
        compiler_params=pltpu.CompilerParams(
            collective_id=collective_id, has_side_effects=True, vmem_limit_bytes=48 * 2**20
        ),
        cost_estimate=pl.CostEstimate(flops=0, bytes_accessed=40 * sent, transcendentals=0),
    )(*[a for a, _, _ in both], gain)


def nt_dot(a, b):
    return lax.dot_general(a, b, (((1,), (1,)), ((), ())), preferred_element_type=jnp.float32)


def up_kernel(
    own_rows, pairs, x_ref, route_ref, g_ref, u_ref, sg_ref, su_ref, hid_ref, go_ref, uo_ref, sgo_ref, suo_ref, inv_ref
):
    p = pl.program_id(0)
    parts, rows, width = x_ref.shape
    d = parts * width
    topk = route_ref.shape[1] // 2
    me = lax.axis_index("fs")

    @pl.when(p == 0)
    def _():
        total = jnp.zeros((rows, 1), jnp.float32)
        for i in range(parts):
            x = x_ref[i].astype(jnp.float32)
            total = total + jnp.sum(x * x, axis=1, keepdims=True)
        inv_ref[...] = jnp.broadcast_to(lax.rsqrt(total / d + norm_eps), inv_ref.shape)
        sgo_ref[...] = sg_ref[...]
        suo_ref[...] = su_ref[...]

    def hidden(g, u):
        acc = None
        for i in range(parts):
            cols = slice(i * width, (i + 1) * width)
            both = jnp.concatenate([g[:, cols], u[:, cols]], axis=0)
            term = nt_dot(x_ref[i], both)
            acc = term if acc is None else acc + term
        half = acc.shape[1] // 2
        gate = acc[:, :half] * inv_ref[:, :1]
        up = acc[:, half:] * inv_ref[:, :1]
        return gate / (1.0 + jnp.exp(-gate)) * up

    @pl.when(p < pairs)
    def _():
        g, u = g_ref[...], u_ref[...]
        go_ref[...] = g
        uo_ref[...] = u
        h = hidden(g.reshape(-1, d), u.reshape(-1, d))
        per = h.shape[1] // 2
        lane = lax.broadcasted_iota(jnp.int32, h.shape, 1)
        expert = (me * (2 * pairs) + 2 * p + jnp.where(lane >= per, 1, 0)).astype(jnp.float32)
        weight = jnp.zeros(h.shape, jnp.float32)
        for k in range(topk):
            weight = weight + jnp.where(
                route_ref[:, k : k + 1] == expert, route_ref[:, topk + k : topk + k + 1], 0.0
            )
        hid_ref[...] = (h * weight).astype(jnp.bfloat16)[None]

    @pl.when(p == pairs)
    def _():
        h = hidden(sg_ref[...], su_ref[...])
        row = lax.broadcasted_iota(jnp.int32, h.shape, 0)
        mine = (row >= me * own_rows) & (row < (me + 1) * own_rows)
        h = jnp.where(mine, h, 0.0).astype(jnp.bfloat16)
        hid_ref[...] = jnp.concatenate([h, jnp.zeros_like(h)], axis=1)[None]


def up_call(own_rows, x, route, gate, up, sg, su):
    experts, hl, d = gate.shape
    pairs = experts // 2
    parts, rows, width = x.shape
    whole = pl.BlockSpec(memory_space=pltpu.VMEM)
    pair_spec = pl.BlockSpec((2, hl, d), lambda p: (jnp.minimum(p, pairs - 1), 0, 0))
    return pl.pallas_call(
        functools.partial(up_kernel, own_rows, pairs),
        grid=(pairs + 1,),
        out_shape=(
            jax.ShapeDtypeStruct((pairs + 1, rows, 2 * hl), jnp.bfloat16),
            jax.ShapeDtypeStruct(gate.shape, gate.dtype),
            jax.ShapeDtypeStruct(up.shape, up.dtype),
            jax.ShapeDtypeStruct(sg.shape, sg.dtype),
            jax.ShapeDtypeStruct(su.shape, su.dtype),
        ),
        in_specs=[whole, whole, pair_spec, pair_spec, whole, whole],
        out_specs=(
            pl.BlockSpec((1, rows, 2 * hl), lambda p: (p, 0, 0)),
            pair_spec,
            pair_spec,
            whole,
            whole,
        ),
        scratch_shapes=[pltpu.VMEM((rows, 128), jnp.float32)],
        compiler_params=pltpu.CompilerParams(vmem_limit_bytes=56 * 2**20),
        cost_estimate=pl.CostEstimate(
            flops=4 * rows * d * hl * (experts + 1), bytes_accessed=8 * gate.size, transcendentals=0
        ),
    )(x, route, gate, up, sg, su)


def down_kernel(hid_ref, d_ref, sd_ref, out_ref, do_ref, sdo_ref, acc_ref):
    i = pl.program_id(0)
    d = d_ref[...]
    do_ref[...] = d
    sd = sd_ref[...]
    sdo_ref[...] = sd
    pairs = hid_ref.shape[1] - 1
    hl = sd.shape[0]
    total = jnp.dot(
        hid_ref[0, pairs][:, :hl], sd, preferred_element_type=jnp.float32
    )
    for p in range(pairs):
        total = total + jnp.dot(
            hid_ref[0, p], d[2 * p : 2 * p + 2].reshape(2 * hl, -1), preferred_element_type=jnp.float32
        )

    @pl.when(i == 0)
    def _():
        acc_ref[...] = total

    @pl.when(i > 0)
    def _():
        acc_ref[...] += total

    @pl.when(i == pl.num_programs(0) - 1)
    def _():
        out_ref[...] = acc_ref[...].astype(jnp.bfloat16)


def down_call(hid, down, sd):
    parts, blocks, rows, _ = hid.shape
    experts, h, d = down.shape
    hl = h // parts
    d_spec = pl.BlockSpec((experts, hl, d), lambda i: (0, i, 0))
    sd_spec = pl.BlockSpec((hl, d), lambda i: (i, 0))
    return pl.pallas_call(
        down_kernel,
        grid=(parts,),
        out_shape=(
            jax.ShapeDtypeStruct((rows, d), jnp.bfloat16),
            jax.ShapeDtypeStruct(down.shape, down.dtype),
            jax.ShapeDtypeStruct(sd.shape, sd.dtype),
        ),
        in_specs=[pl.BlockSpec((1, blocks, rows, hid.shape[3]), lambda i: (i, 0, 0, 0)), d_spec, sd_spec],
        out_specs=(pl.BlockSpec((rows, d), lambda i: (0, 0)), d_spec, sd_spec),
        scratch_shapes=[pltpu.VMEM((rows, d), jnp.float32)],
        compiler_params=pltpu.CompilerParams(vmem_limit_bytes=48 * 2**20),
        cost_estimate=pl.CostEstimate(flops=2 * rows * d * experts * h, bytes_accessed=6 * down.size, transcendentals=0),
    )(hid, down, sd)


def body(
    n,
    tokens,
    expert_ids,
    affinity,
    norm_gain,
    gate_train,
    up_train,
    down_train,
    shared_gate_train,
    shared_up_train,
    shared_down_train,
):
    own_rows = tokens.shape[0]
    route_weight = routed_scale * affinity / jnp.sum(affinity, axis=1, keepdims=True)
    route = jnp.concatenate([expert_ids.astype(jnp.float32), route_weight], axis=1)
    route = lax.all_gather(route, "fs", axis=0, tiled=True)
    columns = lax.all_gather(tokens, "fs", axis=0, tiled=True)
    gain, columns, route = lax.optimization_barrier((norm_gain[None, :], columns, route))
    x = lax.all_gather(columns, "tp", axis=0)
    gate, up, sg, su, sd = exchange(
        n,
        [(gate_train, 2, True), (up_train, 2, True)],
        [(shared_gate_train, 1, True), (shared_up_train, 1, True), (shared_down_train, 0, False)],
        gain,
        0,
    )
    hid, gate_serve, up_serve, shared_gate_serve, shared_up_serve = up_call(own_rows, x, route, gate, up, sg, su)
    down_in, hid = lax.optimization_barrier((down_train, hid))
    every = lax.all_gather(hid, "tp", axis=0)
    (down,) = exchange(n, [(down_in, 1, False)], [], gain, 1)
    part, down_serve, shared_down_serve = down_call(every, down, sd)
    part = lax.all_to_all(part.reshape(n, own_rows, -1), "fs", split_axis=0, concat_axis=0, tiled=True)
    mixed = jnp.sum(part.astype(jnp.float32), axis=0).astype(jnp.bfloat16)
    return (
        mixed,
        gate_serve,
        up_serve,
        down_serve,
        shared_gate_serve,
        shared_up_serve,
        shared_down_serve,
    )


def solution(mesh):
    return jax.shard_map(
        functools.partial(body, mesh.shape["fs"]),
        mesh=mesh,
        in_specs=(
            P("fs", "tp"),
            P("fs", None),
            P("fs", None),
            P("fs"),
            P(None, "tp", "fs"),
            P(None, "tp", "fs"),
            P(None, "fs", "tp"),
            P("tp", "fs"),
            P("tp", "fs"),
            P("fs", "tp"),
        ),
        out_specs=(
            P("fs", "tp"),
            P("fs", "tp", None),
            P("fs", "tp", None),
            P("fs", None, "tp"),
            P("tp", None),
            P("tp", None),
            P(None, "tp"),
        ),
        check_vma=False,
    )
```

time: 511 us -> 387 us (0.76)
  Pallas kernels: 0 us -> 327 us
  blocking collectives: 192 us -> 34.7 us
  waiting for transfers between devices: 99.2 us -> 1.16 us
  local copies, waits for them, and re-layouts: 102 us -> 5.23 us
  other arithmetic: 51.4 us -> 2.84 us
  matrix products: 31.6 us -> 0 us
  starting transfers between devices: 18.5 us -> 0.08 us
    pallas_call x0 -> x4, Pallas kernels: none -> 327 us  [the longest x2 289 us: exchange(): pl.pallas_call(functools.partial(exchange_kernel, n, [(c, g) for _, c, g...]
    all_to_all x2 -> x1, blocking collectives: 130 us -> 12.4 us  [body(): lax.all_to_all(part.reshape(n, own_rows, -1), 'fs', split_axis=0, concat_...]
    all_to_all x4 -> x0, waiting for transfers between devices: 98.4 us -> none  [the longest x1 55.3 us: body(): lax.all_to_all(gate_send, 'fs', split_axis=0, concat_axis=2, tiled=True)]
    all_to_all x7 -> x0, local copies, waits for them, and re-layouts: 63.1 us -> none  [the longest x2 25.4 us: body(): lax.all_to_all(gate_send, 'fs', split_axis=0, concat_axis=2, tiled=True)]
    all_gather x4 -> x2, blocking collectives: 62.6 us -> 22.4 us  [the longest x1 11.2 us: body(): columns = lax.all_gather(tokens, 'fs', axis=0, tiled=True)]
    dot_general x6 -> x0, matrix products: 31.6 us -> none  [the longest x1 12 us: body(): jnp.einsum('erd,ehd->erh', piece, up_serve, preferred_element_type=jnp.fl...]
    convert_element_type x7 -> x1, other arithmetic: 29 us -> 0.69 us  [body(): expert_ids.astype(jnp.float32)]
    all_to_all x4 -> x0, starting transfers between devices: 18.3 us -> none  [the longest x1 5.83 us: body(): lax.all_to_all(gate_send, 'fs', split_axis=0, concat_axis=2, tiled=True)]
  transfers between devices with their start and end apart: 7 -> 2, of which waited for: 2 -> 1; matrix products, arithmetic and copies ran while one was open for 26% -> 0% of each run, Pallas kernels for 0% -> 75%
where the time goes in v1:
time: 387 us; the launch traced here: 385 us
  Pallas kernels  327 us (84%)
  blocking collectives  34.7 us (9%)
  between operations  14.1 us (4%)
  local copies, waits for them, and re-layouts  5.23 us (1%)
    pallas_call x2, Pallas kernels, exchange(): pl.pallas_call(functools.partial(exchange_kernel, n, [(c, g) for _, c, g...  289 us
    pallas_call x1, Pallas kernels, up_call(): pl.pallas_call(functools.partial(up_kernel, own_rows, pairs), grid=(pairs...  22 us
    pallas_call x1, Pallas kernels, down_call(): pl.pallas_call(down_kernel, grid=(parts,), out_shape=(jax.ShapeDtypeStruc...  16.2 us
    all_to_all x1, blocking collectives, body(): lax.all_to_all(part.reshape(n, own_rows, -1), 'fs', split_axis=0, concat_...  12.4 us
    all_gather x1, blocking collectives, body(): columns = lax.all_gather(tokens, 'fs', axis=0, tiled=True)  11.2 us
    all_gather x1, blocking collectives, body(): route = lax.all_gather(route, 'fs', axis=0, tiled=True)  11.2 us
  transfers between devices with their start and end apart: 2, of which 1 were waited for; matrix products, arithmetic and copies ran while one was open for 0% of the time, Pallas kernels for 75%

profile of v1, /device:TPU:0, one launch (start us, length us, event | category | flops | bytes accessed | tf_op | source)
XLA Modules:
  0.0 385.5 jit_solution(17763336013861767394)
XLA Ops:
  7.2 0.0 all-gather.5.cloned.1.call-start
  7.2 0.7 reduce_sum.21
  7.9 0.7 multiply_divide_fusion
  8.6 0.7 convert_element_type.2
  9.3 0.1 copy.21
  9.4 11.2 %all_gather.19.route_ref = f32[512,16]{1,0:T(8,128)} all-gather(f32[128,16]{1,0:T(8,128)S(1)} %copy.21), channel_id=1, replica_groups=mesh['fs'=4,'tp'=8] {'fs'}, dimensions={0}, use_global_device_ids=true | all-gather | bytes 40960 | tf_op jit(solution)/shard_map/all_gather | solution.py:328
  20.6 11.2 %all_gather.18 = bf16[512,512]{1,0:T(8,128)(2,1)} all-gather(bf16[128,512]{1,0:T(8,128)(2,1)} %param.10), channel_id=1, replica_groups=mesh['fs'=4,'tp'=8] {'fs'}, dimensions={0}, use_global_device_ids=true | all-gather | bytes 655360 | tf_op jit(solution)/shard_map/all_gather | solution.py:329
  31.8 0.0 all-gather.5.cloned.1.call-update
  31.8 0.0 all-gather.7.cloned.1.call-start
  31.8 0.0 copy-start
  31.9 0.9 copy-done
  32.8 0.0 copy-start.1
  32.8 0.9 copy-done.1
  33.7 0.0 copy-start.2
  33.7 0.9 copy-done.2
  34.7 0.0 copy-start.3
  34.7 0.7 copy-done.3
  35.4 198.7 %shard_map.153 = (bf16[16,64,4096]{2,1,0:T(8,128)(2,1)}, bf16[16,64,4096]{2,1,0:T(8,128)(2,1)}, bf16[64,4096]{1,0:T(8,128)(2,1)S(1)}, bf16[64,4096]{1,0:T(8,128)(2,1)S(1)}, bf16[512,512]{1,0:T(8,128)(2,1)S(1)}) custom-call(f32[64,64,1024]{2,1,0:T(8,128)} %refs_0_.1, f32[64,64,1024]{2,1,0:T(8,128)} %refs_1_.1, f32[64,1024]{1,0:T(8,128)S(1)} %copy-done, ...), custom_call_target="tpu_custom_call" | custom-call | bytes 503316480 | tf_op jit(solution)/shard_map/pallas_call | solution.py:149
  234.1 0.0 copy-start.5
  234.1 0.8 copy-done.5
  234.9 0.0 copy-start.6
  234.9 0.8 copy-done.6
  235.7 0.0 all-gather.5.cloned.1.call-done
  235.7 0.0 copy-start.4
  235.7 22.0 %shard_map.154 = (bf16[9,512,128]{2,1,0:T(8,128)(2,1)}, bf16[16,64,4096]{2,1,0:T(8,128)(2,1)}, bf16[16,64,4096]{2,1,0:T(8,128)(2,1)}, bf16[64,4096]{1,0:T(8,128)(2,1)}, bf16[64,4096]{1,0:T(8,128)(2,1)}) custom-call(bf16[8,512,512]{2,1,0:T(8,128)(2,1)} %bitcast.8, f32[512,16]{1,0:T(8,128)} %all_gather.19.route_ref, ...), custom_call_target="tpu_custom_call" | custom-call | flops 9126805504 | bytes 33554432 | tf_op jit(solution)/shard_map/pallas_call | solution.py:235
  257.7 0.0 all-gather.7.cloned.1.call-update
  257.7 0.0 copy-done.4
  257.7 90.5 %shard_map.155.d_ref = bf16[16,512,512]{2,1,0:T(8,128)(2,1)} custom-call(f32[64,128,512]{2,1,0:T(8,128)} %refs_0_.2, f32[1,1024]{1,0:T(1,128)S(1)} %bitcast.6), custom_call_target="tpu_custom_call" | custom-call | bytes 251658240 | tf_op jit(solution)/shard_map/pallas_call | solution.py:149
  348.2 1.1 all-gather.7.cloned.1.call-done
  349.3 16.2 %shard_map.156 = (bf16[512,512]{1,0:T(8,128)(2,1)S(1)}, bf16[16,512,512]{2,1,0:T(8,128)(2,1)}, bf16[512,512]{1,0:T(8,128)(2,1)}) custom-call(bf16[8,9,512,128]{3,2,1,0:T(8,128)(2,1)} %bitcast.7, bf16[16,512,512]{2,1,0:T(8,128)(2,1)} %shard_map.155.d_ref, bf16[512,512]{1,0:T(8,128)(2,1)S(1)} %get-tuple-element.35.sd_ref), custom_call_target="tpu_custom_call" | custom-call | flops 4294967296 | bytes 25165824 | tf_op jit(solution)/shard_map/pallas_call | solution.py:296
  365.5 12.4 %all_to_all.5 = bf16[4,128,512]{2,1,0:T(8,128)(2,1)S(1)} all-to-all(bf16[4,128,512]{2,1,0:T(8,128)(2,1)S(1)} %bitcast.4), channel_id=1, replica_groups=mesh['fs'=4,'tp'=8] {'fs'}, dimensions={0} | all-to-all | bytes 1048576 | tf_op jit(solution)/shard_map/all_to_all | solution.py:344
  377.9 0.7 reduce_sum.22
  (1 shorter events, 0.0 us)
Async XLA Ops:
  7.2 228.5 %all-gather.5.cloned.1.call-start = ((), (), s32[]{:S(2)}) async-start(), calls=%async_computation.1 | async-start | bytes 4718592 | tf_op jit(solution)/shard_map/all_gather | solution.py:331
  31.8 317.5 %all-gather.7.cloned.1.call-start = ((), (), s32[]{:S(2)}) async-start(), calls=%async_computation.2 | async-start | bytes 10616832 | tf_op jit(solution)/shard_map/all_gather | solution.py:341
  31.8 1.0 copy-start
  32.8 0.9 copy-start.1
  33.7 0.9 copy-start.2
  34.7 0.7 copy-start.3
  234.1 0.8 copy-start.5
  234.9 0.8 copy-start.6
  235.7 22.0 %copy-start.4 = (f32[1024]{0:T(1024)S(1)}, f32[1024]{0:T(1024)}, u32[]{:S(2)}) copy-start(f32[1024]{0:T(1024)} %param.13) | copy-start | bytes 12292
Sparse Core Ops, SparseCore 0:
  31.9 47.2 all-gather.4
  257.8 91.4 all-gather.6

commit v2 on v1

--- a/solution.py
+++ b/solution.py
@@ -13,22 +13,89 @@
 routed_scale = 2.5
 
 
-def exchange_kernel(n, specs, nsmall, *refs):
+def exchange_kernel(n, ntp, specs, nsmall, *refs):
     nw = len(specs)
     nbig = nw - nsmall
+    extra = 2 if ntp else 0
     ins = refs[:nw]
     gain_ref = refs[nw]
-    outs = refs[nw + 1 : 2 * nw + 1]
-    scr = list(refs[2 * nw + 1 :])
+    refs = refs[nw + 1 :]
+    if ntp:
+        tok_ref, route_ref = refs[:2]
+    outs = refs[extra : extra + nw]
+    if ntp:
+        x_ref, routes_ref = refs[extra + nw : 2 * extra + nw]
+    scr = list(refs[2 * extra + nw :])
     fbuf, lsem, ssem, rsem, osem = scr[:5]
     bufs = scr[5:]
     me = lax.axis_index("fs")
     dest = [lax.rem(me + k, n) for k in range(n)]
+    if ntp:
+        cols, tsem, zsem, zrsem, zosem = scr[-5:]
+        tp = lax.axis_index("tp")
+        tdest = [lax.rem(tp + k, ntp) for k in range(ntp)]
 
     barrier = pltpu.get_barrier_semaphore()
     for k in range(1, n):
         pl.semaphore_signal(barrier, inc=1, device_id={"fs": dest[k]}, device_id_type=MESH)
-    pl.semaphore_wait(barrier, n - 1)
+    for k in range(1, ntp):
+        pl.semaphore_signal(barrier, inc=1, device_id={"tp": tdest[k]}, device_id_type=MESH)
+    pl.semaphore_wait(barrier, n - 1 + max(ntp - 1, 0))
+
+    def token_copy(k, source):
+        rows = tok_ref.shape[0]
+        return pltpu.make_async_remote_copy(
+            src_ref=tok_ref,
+            dst_ref=cols.at[pl.ds(pl.multiple_of(source * rows, rows), rows)],
+            send_sem=tsem.at[0, k],
+            recv_sem=tsem.at[1, k],
+            device_id={"fs": dest[k]},
+            device_id_type=MESH,
+        )
+
+    def route_copy(k, source):
+        rows = route_ref.shape[0]
+        return pltpu.make_async_remote_copy(
+            src_ref=route_ref,
+            dst_ref=routes_ref.at[pl.ds(pl.multiple_of(source * rows, rows), rows)],
+            send_sem=tsem.at[2, k],
+            recv_sem=tsem.at[3, k],
+            device_id={"fs": dest[k]},
+            device_id_type=MESH,
+        )
+
+    def own_token_copy():
+        rows = tok_ref.shape[0]
+        return pltpu.make_async_copy(
+            tok_ref, cols.at[pl.ds(pl.multiple_of(me * rows, rows), rows)], tsem.at[0, 0]
+        )
+
+    def own_route_copy():
+        rows = route_ref.shape[0]
+        return pltpu.make_async_copy(
+            route_ref, routes_ref.at[pl.ds(pl.multiple_of(me * rows, rows), rows)], tsem.at[2, 0]
+        )
+
+    def column_part(source):
+        width = cols.shape[1]
+        return x_ref.at[:, pl.ds(pl.multiple_of(source * width, width), width)]
+
+    def column_copy(k, source):
+        return pltpu.make_async_remote_copy(
+            src_ref=cols,
+            dst_ref=column_part(source),
+            send_sem=zsem.at[k],
+            recv_sem=zrsem.at[k],
+            device_id={"tp": tdest[k]},
+            device_id_type=MESH,
+        )
+
+    if ntp:
+        for k in range(1, n):
+            token_copy(k, me).start()
+            route_copy(k, me).start()
+        own_token_copy().start()
+        own_route_copy().start()
 
     def place(w, who, first, count):
         cut, _ = specs[w]
@@ -102,6 +169,13 @@
             return carry
 
         lax.fori_loop(0, steps, step, 0)
+        if ntp and w == 0:
+            for k in range(1, n):
+                token_copy(k, lax.rem(me + n - k, n)).wait()
+            own_token_copy().wait()
+            for k in range(1, ntp):
+                column_copy(k, tp).start()
+            pltpu.make_async_copy(cols, column_part(tp), zosem).start()
     for s in small:
         for k in order[:-1]:
             remote(s, k, bufs[s], 0, 0).start()
@@ -123,9 +197,16 @@
             ).wait()
         own = bufs[w].at[0] if big else bufs[w]
         pltpu.make_async_copy(own, place(w, me, 0, local), osem.at[w]).wait()
-
-
-def exchange(n, weights, smalls, gain, collective_id):
+    if ntp:
+        for k in range(1, n):
+            route_copy(k, lax.rem(me + n - k, n)).wait()
+        own_route_copy().wait()
+        for k in range(1, ntp):
+            column_copy(k, lax.rem(tp + ntp - k, ntp)).wait()
+        pltpu.make_async_copy(cols, column_part(tp), zosem).wait()
+
+
+def exchange(n, ntp, weights, smalls, gain, tokens, collective_id):
     both = weights + smalls
     outs, bufs = [], []
     for a, cut, _ in weights:
@@ -145,12 +226,27 @@
     chunk = 2 if local % 2 == 0 else 1
     sent = sum(2 * a.size * (n - 1) // n for a, _, _ in weights)
     nw = len(both)
-    any_spec = pl.BlockSpec(memory_space=pl.ANY)
+    any_spec = pl.BlockSpec(memory_space=pltpu.HBM)
+    more, sems = [], []
+    if ntp:
+        (t, cols), (r, lanes) = tokens[0].shape, tokens[1].shape
+        outs += [
+            jax.ShapeDtypeStruct((n * t, ntp * cols), jnp.bfloat16),
+            jax.ShapeDtypeStruct((n * r, lanes), jnp.float32),
+        ]
+        sems = [
+            pltpu.VMEM((n * t, cols), jnp.bfloat16),
+            pltpu.SemaphoreType.DMA((4, n)),
+            pltpu.SemaphoreType.DMA((ntp,)),
+            pltpu.SemaphoreType.DMA((ntp,)),
+            pltpu.SemaphoreType.DMA,
+        ]
+        more = list(tokens)
     return pl.pallas_call(
-        functools.partial(exchange_kernel, n, [(c, g) for _, c, g in both], len(smalls)),
+        functools.partial(exchange_kernel, n, ntp, [(c, g) for _, c, g in both], len(smalls)),
         out_shape=tuple(outs),
-        in_specs=[any_spec] * nw + [pl.BlockSpec(memory_space=pltpu.VMEM)],
-        out_specs=(any_spec,) * nw,
+        in_specs=[any_spec] * nw + [pl.BlockSpec(memory_space=pltpu.VMEM)] + [any_spec] * len(more),
+        out_specs=(any_spec,) * (nw + len(more)),
         scratch_shapes=[
             pltpu.VMEM((n, chunk, *weights[0][0].shape[1:]), jnp.float32),
             pltpu.SemaphoreType.DMA((n,)),
@@ -158,12 +254,13 @@
             pltpu.SemaphoreType.DMA((nw, n)),
             pltpu.SemaphoreType.DMA((nw,)),
             *bufs,
+            *sems,
         ],
         compiler_params=pltpu.CompilerParams(
             collective_id=collective_id, has_side_effects=True, vmem_limit_bytes=48 * 2**20
         ),
         cost_estimate=pl.CostEstimate(flops=0, bytes_accessed=40 * sent, transcendentals=0),
-    )(*[a for a, _, _ in both], gain)
+    )(*[a for a, _, _ in both], gain, *more)
 
 
 def nt_dot(a, b):
@@ -171,31 +268,26 @@
 
 
 def up_kernel(
-    own_rows, pairs, x_ref, route_ref, g_ref, u_ref, sg_ref, su_ref, hid_ref, go_ref, uo_ref, sgo_ref, suo_ref, inv_ref
+    own_rows, pairs, group, x_ref, route_ref, g_ref, u_ref, sg_ref, su_ref, hid_ref, go_ref, uo_ref, sgo_ref, suo_ref, inv_ref
 ):
     p = pl.program_id(0)
-    parts, rows, width = x_ref.shape
-    d = parts * width
+    rows, d = x_ref.shape
     topk = route_ref.shape[1] // 2
     me = lax.axis_index("fs")
 
     @pl.when(p == 0)
     def _():
         total = jnp.zeros((rows, 1), jnp.float32)
-        for i in range(parts):
-            x = x_ref[i].astype(jnp.float32)
+        width = 512
+        for i in range(0, d, width):
+            x = x_ref[:, i : i + width].astype(jnp.float32)
             total = total + jnp.sum(x * x, axis=1, keepdims=True)
         inv_ref[...] = jnp.broadcast_to(lax.rsqrt(total / d + norm_eps), inv_ref.shape)
         sgo_ref[...] = sg_ref[...]
         suo_ref[...] = su_ref[...]
 
     def hidden(g, u):
-        acc = None
-        for i in range(parts):
-            cols = slice(i * width, (i + 1) * width)
-            both = jnp.concatenate([g[:, cols], u[:, cols]], axis=0)
-            term = nt_dot(x_ref[i], both)
-            acc = term if acc is None else acc + term
+        acc = nt_dot(x_ref[...], jnp.concatenate([g, u], axis=0))
         half = acc.shape[1] // 2
         gate = acc[:, :half] * inv_ref[:, :1]
         up = acc[:, half:] * inv_ref[:, :1]
@@ -207,15 +299,15 @@
         go_ref[...] = g
         uo_ref[...] = u
         h = hidden(g.reshape(-1, d), u.reshape(-1, d))
-        per = h.shape[1] // 2
+        per = h.shape[1] // group
         lane = lax.broadcasted_iota(jnp.int32, h.shape, 1)
-        expert = (me * (2 * pairs) + 2 * p + jnp.where(lane >= per, 1, 0)).astype(jnp.float32)
+        expert = (me * (group * pairs) + group * p + lane // per).astype(jnp.float32)
         weight = jnp.zeros(h.shape, jnp.float32)
         for k in range(topk):
             weight = weight + jnp.where(
                 route_ref[:, k : k + 1] == expert, route_ref[:, topk + k : topk + k + 1], 0.0
             )
-        hid_ref[...] = (h * weight).astype(jnp.bfloat16)[None]
+        hid_ref[...] = (h * weight).astype(jnp.bfloat16)
 
     @pl.when(p == pairs)
     def _():
@@ -223,20 +315,21 @@
         row = lax.broadcasted_iota(jnp.int32, h.shape, 0)
         mine = (row >= me * own_rows) & (row < (me + 1) * own_rows)
         h = jnp.where(mine, h, 0.0).astype(jnp.bfloat16)
-        hid_ref[...] = jnp.concatenate([h, jnp.zeros_like(h)], axis=1)[None]
+        hid_ref[...] = jnp.concatenate([h] + [jnp.zeros_like(h)] * (group - 1), axis=1)
 
 
 def up_call(own_rows, x, route, gate, up, sg, su):
     experts, hl, d = gate.shape
-    pairs = experts // 2
-    parts, rows, width = x.shape
+    group = min(experts, max(1, 128 // hl))
+    pairs = experts // group
+    rows = x.shape[0]
     whole = pl.BlockSpec(memory_space=pltpu.VMEM)
-    pair_spec = pl.BlockSpec((2, hl, d), lambda p: (jnp.minimum(p, pairs - 1), 0, 0))
+    pair_spec = pl.BlockSpec((group, hl, d), lambda p: (jnp.minimum(p, pairs - 1), 0, 0))
     return pl.pallas_call(
-        functools.partial(up_kernel, own_rows, pairs),
+        functools.partial(up_kernel, own_rows, pairs, group),
         grid=(pairs + 1,),
         out_shape=(
-            jax.ShapeDtypeStruct((pairs + 1, rows, 2 * hl), jnp.bfloat16),
+            jax.ShapeDtypeStruct((rows, (pairs + 1) * group * hl), jnp.bfloat16),
             jax.ShapeDtypeStruct(gate.shape, gate.dtype),
             jax.ShapeDtypeStruct(up.shape, up.dtype),
             jax.ShapeDtypeStruct(sg.shape, sg.dtype),
@@ -244,7 +337,7 @@
         ),
         in_specs=[whole, whole, pair_spec, pair_spec, whole, whole],
         out_specs=(
-            pl.BlockSpec((1, rows, 2 * hl), lambda p: (p, 0, 0)),
+            pl.BlockSpec((rows, group * hl), lambda p: (0, p)),
             pair_spec,
             pair_spec,
             whole,
@@ -264,15 +357,10 @@
     do_ref[...] = d
     sd = sd_ref[...]
     sdo_ref[...] = sd
-    pairs = hid_ref.shape[1] - 1
     hl = sd.shape[0]
-    total = jnp.dot(
-        hid_ref[0, pairs][:, :hl], sd, preferred_element_type=jnp.float32
-    )
-    for p in range(pairs):
-        total = total + jnp.dot(
-            hid_ref[0, p], d[2 * p : 2 * p + 2].reshape(2 * hl, -1), preferred_element_type=jnp.float32
-        )
+    wide = d.shape[0] * hl
+    total = jnp.dot(hid_ref[0, :, :wide], d.reshape(wide, -1), preferred_element_type=jnp.float32)
+    total += jnp.dot(hid_ref[0, :, wide : wide + hl], sd, preferred_element_type=jnp.float32)
 
     @pl.when(i == 0)
     def _():
@@ -288,7 +376,7 @@
 
 
 def down_call(hid, down, sd):
-    parts, blocks, rows, _ = hid.shape
+    parts, rows, lanes = hid.shape
     experts, h, d = down.shape
     hl = h // parts
     d_spec = pl.BlockSpec((experts, hl, d), lambda i: (0, i, 0))
@@ -301,7 +389,7 @@
             jax.ShapeDtypeStruct(down.shape, down.dtype),
             jax.ShapeDtypeStruct(sd.shape, sd.dtype),
         ),
-        in_specs=[pl.BlockSpec((1, blocks, rows, hid.shape[3]), lambda i: (i, 0, 0, 0)), d_spec, sd_spec],
+        in_specs=[pl.BlockSpec((1, rows, lanes), lambda i: (i, 0, 0)), d_spec, sd_spec],
         out_specs=(pl.BlockSpec((rows, d), lambda i: (0, 0)), d_spec, sd_spec),
         scratch_shapes=[pltpu.VMEM((rows, d), jnp.float32)],
         compiler_params=pltpu.CompilerParams(vmem_limit_bytes=48 * 2**20),
@@ -309,8 +397,57 @@
     )(hid, down, sd)
 
 
+def combine_kernel(n, part_ref, out_ref, landed, ssem, rsem):
+    me = lax.axis_index("fs")
+    rows = out_ref.shape[0]
+    barrier = pltpu.get_barrier_semaphore()
+    for k in range(1, n):
+        pl.semaphore_signal(barrier, inc=1, device_id={"fs": lax.rem(me + k, n)}, device_id_type=MESH)
+    pl.semaphore_wait(barrier, n - 1)
+
+    def block(who):
+        return part_ref.at[pl.ds(pl.multiple_of(who * rows, rows), rows)]
+
+    copies = []
+    for k in range(1, n):
+        to = lax.rem(me + k, n)
+        copy = pltpu.make_async_remote_copy(
+            src_ref=block(to),
+            dst_ref=landed.at[k - 1],
+            send_sem=ssem.at[k - 1],
+            recv_sem=rsem.at[k - 1],
+            device_id={"fs": to},
+            device_id_type=MESH,
+        )
+        copy.start()
+        copies.append(copy)
+    total = block(me)[...].astype(jnp.float32)
+    for k in range(1, n):
+        copies[k - 1].wait()
+        total = total + landed[k - 1].astype(jnp.float32)
+    out_ref[...] = total.astype(out_ref.dtype)
+
+
+def combine(n, part, collective_id):
+    rows, d = part.shape[0] // n, part.shape[1]
+    vmem = pl.BlockSpec(memory_space=pltpu.VMEM)
+    return pl.pallas_call(
+        functools.partial(combine_kernel, n),
+        out_shape=jax.ShapeDtypeStruct((rows, d), part.dtype),
+        in_specs=[vmem],
+        out_specs=vmem,
+        scratch_shapes=[
+            pltpu.VMEM((n - 1, rows, d), part.dtype),
+            pltpu.SemaphoreType.DMA((n - 1,)),
+            pltpu.SemaphoreType.DMA((n - 1,)),
+        ],
+        compiler_params=pltpu.CompilerParams(collective_id=collective_id, has_side_effects=True),
+    )(part)
+
+
 def body(
     n,
+    ntp,
     tokens,
     expert_ids,
     affinity,
@@ -325,24 +462,22 @@
     own_rows = tokens.shape[0]
     route_weight = routed_scale * affinity / jnp.sum(affinity, axis=1, keepdims=True)
     route = jnp.concatenate([expert_ids.astype(jnp.float32), route_weight], axis=1)
-    route = lax.all_gather(route, "fs", axis=0, tiled=True)
-    columns = lax.all_gather(tokens, "fs", axis=0, tiled=True)
-    gain, columns, route = lax.optimization_barrier((norm_gain[None, :], columns, route))
-    x = lax.all_gather(columns, "tp", axis=0)
-    gate, up, sg, su, sd = exchange(
+    gain = norm_gain[None, :]
+    gate, up, sg, su, sd, x, route = exchange(
         n,
+        ntp,
         [(gate_train, 2, True), (up_train, 2, True)],
         [(shared_gate_train, 1, True), (shared_up_train, 1, True), (shared_down_train, 0, False)],
         gain,
+        (tokens, route),
         0,
     )
     hid, gate_serve, up_serve, shared_gate_serve, shared_up_serve = up_call(own_rows, x, route, gate, up, sg, su)
     down_in, hid = lax.optimization_barrier((down_train, hid))
     every = lax.all_gather(hid, "tp", axis=0)
-    (down,) = exchange(n, [(down_in, 1, False)], [], gain, 1)
+    (down,) = exchange(n, 0, [(down_in, 1, False)], [], gain, None, 1)
     part, down_serve, shared_down_serve = down_call(every, down, sd)
-    part = lax.all_to_all(part.reshape(n, own_rows, -1), "fs", split_axis=0, concat_axis=0, tiled=True)
-    mixed = jnp.sum(part.astype(jnp.float32), axis=0).astype(jnp.bfloat16)
+    mixed = combine(n, part, 2)
     return (
         mixed,
         gate_serve,
@@ -356,7 +491,7 @@
 
 def solution(mesh):
     return jax.shard_map(
-        functools.partial(body, mesh.shape["fs"]),
+        functools.partial(body, mesh.shape["fs"], mesh.shape["tp"]),
         mesh=mesh,
         in_specs=(
             P("fs", "tp"),

time: 387 us -> 382 us (0.987)
  blocking collectives: 34.7 us -> 0 us
  Pallas kernels: 327 us -> 355 us
  local copies, waits for them, and re-layouts: 5.23 us -> 9.19 us
    pallas_call x3 -> x4, Pallas kernels: 311 us -> 341 us  [the longest x2 309 us: exchange(): pl.pallas_call(functools.partial(exchange_kernel, n, ntp, [(c, g) for _,...]
    all_gather x2 -> x0, blocking collectives: 22.4 us -> none  [the longest x1 11.2 us: body(): columns = lax.all_gather(tokens, 'fs', axis=0, tiled=True)]
    all_to_all x1 -> x0, blocking collectives: 12.4 us -> none  [body(): lax.all_to_all(part.reshape(n, own_rows, -1), 'fs', split_axis=0, concat_...]
    unnamed x14 -> x21, local copies, waits for them, and re-layouts: 5.13 us -> 9.09 us
  transfers between devices with their start and end apart: 2 -> 1, of which waited for: 1 -> 0; matrix products, arithmetic and copies ran while one was open for 0% -> 0% of each run, Pallas kernels for 75% -> 25%
where the time goes in v2:
time: 382 us; the launch traced here: 380 us
  Pallas kernels  355 us (93%)
  between operations  14.1 us (4%)
  local copies, waits for them, and re-layouts  9.19 us (2%)
    pallas_call x2, Pallas kernels, exchange(): pl.pallas_call(functools.partial(exchange_kernel, n, ntp, [(c, g) for _,...  309 us
    pallas_call x1, Pallas kernels, up_call(): pl.pallas_call(functools.partial(up_kernel, own_rows, pairs, group), grid...  22.1 us
    pallas_call x1, Pallas kernels, down_call(): pl.pallas_call(down_kernel, grid=(parts,), out_shape=(jax.ShapeDtypeStruc...  14.1 us
    pallas_call x1, Pallas kernels, combine(): pl.pallas_call(functools.partial(combine_kernel, n), out_shape=jax.ShapeD...  9.67 us
    unnamed x21, local copies, waits for them, and re-layouts  9.09 us
  transfers between devices with their start and end apart: 1, of which 0 were waited for; matrix products, arithmetic and copies ran while one was open for 0% of the time, Pallas kernels for 25%

profile of v2, /device:TPU:0, one launch (start us, length us, event | category | flops | bytes accessed | tf_op | source)
XLA Modules:
  0.0 380.3 jit_solution(10581684956098815747)
XLA Ops:
  7.2 0.0 all-gather.3.cloned.1.call-start
  7.2 0.7 reduce_sum.9
  7.9 0.7 multiply_divide_fusion
  8.6 0.7 convert_element_type.3
  9.3 0.1 copy.21.refs_7_
  9.4 0.0 copy-start.1
  9.4 0.9 copy-done.1
  10.4 0.0 copy-start.2
  10.4 0.9 copy-done.2
  11.3 0.0 copy-start.3
  11.3 0.9 copy-done.3
  12.3 0.0 copy-start.4
  12.3 0.9 copy-done.4
  13.2 0.0 copy-start.5
  13.2 0.7 copy-done.5
  13.9 214.2 %shard_map.153 = (bf16[16,64,4096]{2,1,0:T(8,128)(2,1)}, bf16[16,64,4096]{2,1,0:T(8,128)(2,1)}, bf16[64,4096]{1,0:T(8,128)(2,1)S(1)}, bf16[64,4096]{1,0:T(8,128)...) custom-call(f32[64,64,1024]{2,1,0:T(8,128)} %refs_0_.1, ...), custom_call_target="tpu_custom_call" | custom-call | bytes 503316480 | tf_op jit(solution)/shard_map/pallas_call | solution.py:245
  228.1 0.0 copy-start.7
  228.1 0.8 copy-done.7
  228.9 0.0 copy-start.8
  228.9 0.8 copy-done.8
  229.7 0.0 copy-start.9
  229.7 0.7 copy-done.9
  230.4 0.0 copy-start.6
  230.4 22.1 %shard_map.154 = (bf16[512,1152]{1,0:T(8,128)(2,1)}, bf16[16,64,4096]{2,1,0:T(8,128)(2,1)}, bf16[16,64,4096]{2,1,0:T(8,128)(2,1)}, bf16[64,4096]{1,0:T(8,128)(2,1)}, bf16[64,4096]{1,0:T(8,128)(2,1)}) custom-call(bf16[512,4096]{1,0:T(8,128)(2,1)} %get-tuple-element.24.x_ref, f32[512,16]{1,0:T(8,128)} %copy-done.9, ...), custom_call_target="tpu_custom_call" | custom-call | flops 9126805504 | bytes 33554432 | tf_op jit(solution)/shard_map/pallas_call | solution.py:328
  252.4 0.0 all-gather.3.cloned.1.call-update
  252.5 0.0 copy-done.6
  252.5 94.8 %shard_map.155.d_ref = bf16[16,512,512]{2,1,0:T(8,128)(2,1)} custom-call(f32[64,128,512]{2,1,0:T(8,128)} %refs_0_.2, f32[1,1024]{1,0:T(1,128)S(1)} %bitcast.3), custom_call_target="tpu_custom_call" | custom-call | bytes 251658240 | tf_op jit(solution)/shard_map/pallas_call | solution.py:245
  347.3 0.0 all-gather.3.cloned.1.call-done
  347.3 14.1 %shard_map.156 = (bf16[512,512]{1,0:T(8,128)(2,1)S(1)}, bf16[16,512,512]{2,1,0:T(8,128)(2,1)}, bf16[512,512]{1,0:T(8,128)(2,1)}) custom-call(bf16[8,512,1152]{2,1,0:T(8,128)(2,1)} %bitcast.4, bf16[16,512,512]{2,1,0:T(8,128)(2,1)} %shard_map.155.d_ref, bf16[512,512]{1,0:T(8,128)(2,1)S(1)} %get-tuple-element.33.sd_ref), custom_call_target="tpu_custom_call" | custom-call | flops 4294967296 | bytes 25165824 | tf_op jit(solution)/shard_map/pallas_call | solution.py:384
  361.4 0.0 copy-start
  361.4 0.8 copy-done
  362.2 9.7 %shard_map.157 = bf16[128,512]{1,0:T(8,128)(2,1)} custom-call(bf16[512,512]{1,0:T(8,128)(2,1)} %copy-done), custom_call_target="tpu_custom_call" | custom-call | tf_op jit(solution)/shard_map/pallas_call | solution.py:434
  371.9 1.6 copy.23
  (1 shorter events, 0.0 us)
Async XLA Ops:
  7.2 340.2 %all-gather.3.cloned.1.call-start = ((), (), s32[]{:S(2)}) async-start(), calls=%async_computation | async-start | bytes 10616832 | tf_op jit(solution)/shard_map/all_gather | solution.py:477
  9.4 1.0 copy-start.1
  10.4 0.9 copy-start.2
  11.3 0.9 copy-start.3
  12.3 0.9 copy-start.4
  13.2 0.7 copy-start.5
  228.1 0.8 copy-start.7
  228.9 0.8 copy-start.8
  229.7 0.7 copy-start.9
  230.4 22.1 %copy-start.6 = (f32[1024]{0:T(1024)S(1)}, f32[1024]{0:T(1024)}, u32[]{:S(2)}) copy-start(f32[1024]{0:T(1024)} %param.13) | copy-start | bytes 12292
  361.4 0.8 copy-start
Sparse Core Ops, SparseCore 0:
  252.6 89.0 all-gather.2

commit v3 on v2

--- a/solution.py
+++ b/solution.py
@@ -257,7 +257,7 @@
             *sems,
         ],
         compiler_params=pltpu.CompilerParams(
-            collective_id=collective_id, has_side_effects=True, vmem_limit_bytes=48 * 2**20
+            collective_id=collective_id, has_side_effects=True, vmem_limit_bytes=60 * 1024 * 1024
         ),
         cost_estimate=pl.CostEstimate(flops=0, bytes_accessed=40 * sent, transcendentals=0),
     )(*[a for a, _, _ in both], gain, *more)
@@ -344,7 +344,7 @@
             whole,
         ),
         scratch_shapes=[pltpu.VMEM((rows, 128), jnp.float32)],
-        compiler_params=pltpu.CompilerParams(vmem_limit_bytes=56 * 2**20),
+        compiler_params=pltpu.CompilerParams(vmem_limit_bytes=60 * 1024 * 1024),
         cost_estimate=pl.CostEstimate(
             flops=4 * rows * d * hl * (experts + 1), bytes_accessed=8 * gate.size, transcendentals=0
         ),
@@ -392,7 +392,7 @@
         in_specs=[pl.BlockSpec((1, rows, lanes), lambda i: (i, 0, 0)), d_spec, sd_spec],
         out_specs=(pl.BlockSpec((rows, d), lambda i: (0, 0)), d_spec, sd_spec),
         scratch_shapes=[pltpu.VMEM((rows, d), jnp.float32)],
-        compiler_params=pltpu.CompilerParams(vmem_limit_bytes=48 * 2**20),
+        compiler_params=pltpu.CompilerParams(vmem_limit_bytes=60 * 1024 * 1024),
         cost_estimate=pl.CostEstimate(flops=2 * rows * d * experts * h, bytes_accessed=6 * down.size, transcendentals=0),
     )(hid, down, sd)
 
@@ -441,7 +441,7 @@
             pltpu.SemaphoreType.DMA((n - 1,)),
             pltpu.SemaphoreType.DMA((n - 1,)),
         ],
-        compiler_params=pltpu.CompilerParams(collective_id=collective_id, has_side_effects=True),
+        compiler_params=pltpu.CompilerParams(collective_id=collective_id, has_side_effects=True, vmem_limit_bytes=60 * 1024 * 1024),
     )(part)
 
 

time: 382 us -> 377 us (0.987)
  local copies, waits for them, and re-layouts: 9.19 us -> 2.3 us
    unnamed x21 -> x1, local copies, waits for them, and re-layouts: 9.09 us -> 1.57 us
where the time goes in v3:
time: 377 us; the launch traced here: 375 us
  Pallas kernels  357 us (95%)
  between operations  14.1 us (4%)
    pallas_call x2, Pallas kernels, exchange(): pl.pallas_call(functools.partial(exchange_kernel, n, ntp, [(c, g) for _,...  311 us
    pallas_call x1, Pallas kernels, up_call(): pl.pallas_call(functools.partial(up_kernel, own_rows, pairs, group), grid...  22.1 us
    pallas_call x1, Pallas kernels, down_call(): pl.pallas_call(down_kernel, grid=(parts,), out_shape=(jax.ShapeDtypeStruc...  14.2 us
    pallas_call x1, Pallas kernels, combine(): pl.pallas_call(functools.partial(combine_kernel, n), out_shape=jax.ShapeD...  9.68 us
  transfers between devices with their start and end apart: 1, of which 0 were waited for; matrix products, arithmetic and copies ran while one was open for 0% of the time, Pallas kernels for 25%

profile of v3, /device:TPU:0, one launch (start us, length us, event | category | flops | bytes accessed | tf_op | source)
XLA Modules:
  0.0 375.2 jit_solution(12895374886632357112)
XLA Ops:
  7.2 0.0 all-gather.3.cloned.1.call-start
  7.2 0.7 reduce_sum.9
  7.9 0.7 multiply_divide_fusion
  8.6 0.7 convert_element_type.3
  9.3 0.7 copy.21.refs_7_
  10.0 215.2 %shard_map.153 = (bf16[16,64,4096]{2,1,0:T(8,128)(2,1)}, bf16[16,64,4096]{2,1,0:T(8,128)(2,1)}, bf16[64,4096]{1,0:T(8,128)(2,1)}, bf16[64,4096]{1,0:T(8,128)(2,1...) custom-call(f32[64,64,1024]{2,1,0:T(8,128)} %refs_0_.1, f32[64,64,1024]{2,1,0:T(8,128)} %refs_1_.1, ...), custom_call_target="tpu_custom_call" | custom-call | bytes 503316480 | tf_op jit(solution)/shard_map/pallas_call | solution.py:245
  225.3 22.1 %shard_map.154 = (bf16[512,1152]{1,0:T(8,128)(2,1)}, bf16[16,64,4096]{2,1,0:T(8,128)(2,1)}, bf16[16,64,4096]{2,1,0:T(8,128)(2,1)}, bf16[64,4096]{1,0:T(8,128)(2,1)}, bf16[64,4096]{1,0:T(8,128)(2,1)}) custom-call(bf16[512,4096]{1,0:T(8,128)(2,1)} %get-tuple-element.24.x_ref, f32[512,16]{1,0:T(8,128)} %get-tuple-element.25.route_ref, ...), custom_call_target="tpu_custom_call" | custom-call | flops 9126805504 | bytes 33554432 | tf_op jit(solution)/shard_map/pallas_call | solution.py:328
  247.3 0.0 all-gather.3.cloned.1.call-update
  247.4 95.5 %shard_map.155.d_ref = bf16[16,512,512]{2,1,0:T(8,128)(2,1)} custom-call(f32[64,128,512]{2,1,0:T(8,128)} %refs_0_.2, f32[1,1024]{1,0:T(1,128)} %bitcast.4), custom_call_target="tpu_custom_call" | custom-call | bytes 251658240 | tf_op jit(solution)/shard_map/pallas_call | solution.py:245
  342.9 0.0 all-gather.3.cloned.1.call-done
  342.9 14.2 %shard_map.156 = (bf16[512,512]{1,0:T(8,128)(2,1)}, bf16[16,512,512]{2,1,0:T(8,128)(2,1)}, bf16[512,512]{1,0:T(8,128)(2,1)}) custom-call(bf16[8,512,1152]{2,1,0:T(8,128)(2,1)} %bitcast.2, bf16[16,512,512]{2,1,0:T(8,128)(2,1)} %shard_map.155.d_ref, bf16[512,512]{1,0:T(8,128)(2,1)} %get-tuple-element.33.sd_ref), custom_call_target="tpu_custom_call" | custom-call | flops 4294967296 | bytes 25165824 | tf_op jit(solution)/shard_map/pallas_call | solution.py:384
  357.1 9.7 %shard_map.157 = bf16[128,512]{1,0:T(8,128)(2,1)} custom-call(bf16[512,512]{1,0:T(8,128)(2,1)} %get-tuple-element.34.part_ref), custom_call_target="tpu_custom_call" | custom-call | tf_op jit(solution)/shard_map/pallas_call | solution.py:434
  366.8 1.6 copy.23
  (1 shorter events, 0.0 us)
Async XLA Ops:
  7.2 335.7 %all-gather.3.cloned.1.call-start = ((), (), s32[]{:S(2)}) async-start(), calls=%async_computation | async-start | bytes 10616832 | tf_op jit(solution)/shard_map/all_gather | solution.py:477
Sparse Core Ops, SparseCore 0:
  247.5 89.0 all-gather.2
